TPU v7x, 32 devices: a whole 2x2x4 slice. The times are simulated.
32 devices in a mesh: sp: 8 (over z, y), tp: 4 (over x, core).
Axes of the slice: x: 2, y: 2, z: 4, core: 2. Of those that a mesh axis runs over, the one named last changes fastest.
Arguments:
- d_out: bfloat16 [4096, 2048], P('sp'), may hold values from -6 to 6
- route_expert: int32 [4096, 2], P('sp'), may hold values from 0 to 7, all different within a row; in each aligned block of 512 rows (0 to 511, 512 to 1023, ...) at most 144 rows name the same one
- route_weight: float32 [4096, 2], P('sp'), may hold values from 0.2 to 1
- expert_inputs: bfloat16 [8, 1152, 2048], P('sp'), may hold values from -6 to 6
- w_gate: bfloat16 [8, 2048, 2816], P('sp', None, 'tp'), may hold values from -0.125 to 0.125
- w_up: bfloat16 [8, 2048, 2816], P('sp', None, 'tp'), may hold values from -0.125 to 0.125
- w_down: bfloat16 [8, 2816, 2048], P('sp', 'tp'), may hold values from -0.109375 to 0.109375
- w_out: bfloat16 [2048, 1024], P(None, 'tp'), may hold values from -0.1875 to 0.1875
- queries: bfloat16 [4096, 4, 128], P('sp', 'tp'), may hold values from -6 to 6
- keys: bfloat16 [4096, 4, 128], P('sp', 'tp'), may hold values from -2 to 2
- values: bfloat16 [4096, 4, 256], P('sp', 'tp'), may hold values from -6 to 6
- log_decay: float32 [4096, 4, 128], P('sp', 'tp'), may hold values from -1 to 0
Outputs:
- grad_gate: bfloat16 [8, 2048, 2816], P('sp', None, 'tp')
- grad_up: bfloat16 [8, 2048, 2816], P('sp', None, 'tp')
- grad_down: bfloat16 [8, 2816, 2048], P('sp', 'tp')
- grad_proj: float32 [2048, 1024], P('sp', 'tp')
- grad_queries: bfloat16 [4096, 4, 128], P('sp', 'tp')
- grad_keys: bfloat16 [4096, 4, 128], P('sp', 'tp')
- grad_values: bfloat16 [4096, 4, 256], P('sp', 'tp')
- grad_log_decay: float32 [4096, 4, 128], P('sp', 'tp')
Inputs may be any that keep to these rules, and one draw needn't show every extreme that they name: `route_expert`: the two experts of a token differ. Among the rows of one device no expert is named more than 144 times, and in every draw some device names some expert exactly 144 times.
All inputs are finite; a program needn't handle non-finite values.
Results may differ from a plain program's by a relative error of at most 0.02.
Values may be sent and summed in bfloat16 or wider, within the bound.
A program may use at most 128 MiB of HBM per device.

v0:
```python
import functools

import jax
import jax.numpy as jnp
from jax import lax
from jax.experimental import pallas as pl
from jax.experimental.pallas import tpu as pltpu
from jax.sharding import PartitionSpec as P

BLK = 64


precise = lax.Precision.HIGHEST


MESH = pl.DeviceIdType.MESH
NN = (((1,), (0,)), ((), ()))
NT = (((1,), (1,)), ((), ()))
TN = (((0,), (0,)), ((), ()))


def mm(a, b, dims):
    return lax.dot_general(a, b, dims, preferred_element_type=jnp.float32)


def triangle(lower):
    rows = lax.broadcasted_iota(jnp.int32, (BLK, BLK), 0)
    cols = lax.broadcasted_iota(jnp.int32, (BLK, BLK), 1)
    return rows >= cols if lower else rows <= cols


def block_sums(mask, x):
    return lax.dot_general(
        mask.astype(jnp.float32), x, NN, precision=precise, preferred_element_type=jnp.float32
    )


def decays(g_ref, rows):
    cumulative = block_sums(triangle(True), g_ref[rows, :])
    middle = cumulative[BLK // 2 - 1 : BLK // 2, :]
    ending = cumulative[BLK - 1 : BLK, :]
    return cumulative, middle, ending


def greet(n, me, tp=None):
    barrier = pltpu.get_barrier_semaphore()
    others = [{"sp": lax.rem(me + k, n)} for k in range(1, n)]
    if tp is not None:
        others += [{"tp": other} for other in tp]
    for other in others:
        pl.semaphore_signal(barrier, inc=1, device_id=other, device_id_type=MESH)
    return barrier, len(others)


def route_kernel(
    n,
    tp,
    cap,
    d_ref,
    expert_ref,
    weight_ref,
    routed_ref,
    slot_ref,
    outbox,
    ssem,
    rsem,
    lsem,
    tsend,
    trecv,
):
    me = lax.axis_index("sp")
    col = lax.axis_index("tp")
    partner = col + 1 - 2 * lax.rem(col, 2)
    far = [lax.rem(col + 2 * s, tp) for s in range(1, tp // 2)]
    barrier, greeted = greet(n, me, [partner] + far)
    tokens = d_ref.shape[0]
    quarter = outbox.shape[2]
    start = pl.multiple_of(lax.axis_index("tp") * quarter, quarter)
    own = d_ref[:, pl.ds(start, quarter)].astype(jnp.float32)
    kinds = lax.broadcasted_iota(jnp.int32, (n, tokens), 0)
    named = [(kinds == expert_ref[j : j + 1, :]).astype(jnp.float32) for j in range(2)]
    earlier = lax.broadcasted_iota(jnp.int32, (tokens, tokens), 0) < lax.broadcasted_iota(
        jnp.int32, (tokens, tokens), 1
    )
    before = mm((named[0] + named[1]).astype(jnp.bfloat16), earlier.astype(jnp.bfloat16), NN)
    scaled = []
    slots = []
    for j in range(2):
        rank = jnp.sum(before * named[j], axis=0, keepdims=True).astype(jnp.int32)
        slots.append(expert_ref[j : j + 1, :] * cap + rank)
        slot_ref[j : j + 1, :] = slots[j]
        scaled.append((own * weight_ref[:, j : j + 1]).astype(jnp.bfloat16))
    places = lax.broadcasted_iota(jnp.int32, (cap, tokens), 0)
    for e in range(n):
        rows = jnp.zeros((cap, quarter), jnp.float32)
        for j in range(2):
            picks = (slots[j] - e * cap == places).astype(jnp.float32).astype(jnp.bfloat16)
            rows = rows + mm(picks, scaled[j], NN)
        outbox[e] = rows.astype(jnp.bfloat16)
    pl.semaphore_wait(barrier, greeted)

    def place(row, column):
        return routed_ref.at[row, :, pl.ds(pl.multiple_of(column * quarter, quarter), quarter)]

    copies = []
    for k in range(1, n):
        peer = lax.rem(me + k, n)
        copies.append(
            pltpu.make_async_remote_copy(
                src_ref=outbox.at[peer],
                dst_ref=place(me, col),
                send_sem=ssem.at[k - 1],
                recv_sem=rsem.at[k - 1],
                device_id={"sp": peer},
                device_id_type=MESH,
            )
        )
        copies[-1].start()
    stays = pltpu.make_async_copy(outbox.at[me], place(me, col), lsem)
    stays.start()

    def send(k, column, slot, target):
        row = lax.rem(me - k + n, n)
        return pltpu.make_async_remote_copy(
            src_ref=place(row, column),
            dst_ref=place(row, column),
            send_sem=tsend.at[k, slot],
            recv_sem=trecv.at[k, slot],
            device_id={"tp": target},
            device_id_type=MESH,
        )

    across, beside, passed = [], [], []

    def pass_on(k):
        for s in range(len(far)):
            across[k][s].wait_recv()
            column = lax.rem(col - 2 * (s + 1) + tp, tp)
            passed.append(send(k, column, tp // 2 + s, partner))
            passed[-1].start()

    for k in range(n):
        if k == 0:
            stays.wait()
        else:
            copies[k - 1].wait_recv()
        across.append([send(k, col, s + 1, far[s]) for s in range(len(far))])
        for copy in across[k]:
            copy.start()
        beside.append(send(k, col, 0, partner))
        beside[k].start()
        if k > 1:
            pass_on(k - 2)
    for k in range(max(n - 2, 0), n):
        pass_on(k)
    for copy in copies:
        copy.wait_send()
    for row in across:
        for copy in row:
            copy.wait_send()
    for copy in beside + passed:
        copy.wait()


def exchange(n, me, source, target, ssem, rsem, lsem):
    copies = []
    for k in range(1, n):
        peer = lax.rem(me + k, n)
        copies.append(
            pltpu.make_async_remote_copy(
                src_ref=source.at[peer],
                dst_ref=target.at[me],
                send_sem=ssem.at[k - 1],
                recv_sem=rsem.at[k - 1],
                device_id={"sp": peer},
                device_id_type=MESH,
            )
        )
    for copy in copies:
        copy.start()
    stays = pltpu.make_async_copy(source.at[me], target.at[me], lsem)
    stays.start()
    stays.wait()
    for copy in copies:
        copy.wait()


def return_kernel(
    n, tp, cap, sums_ref, slot_ref, d_ref, gathered_ref, back, ssem, rsem, lsem, tsend, trecv
):
    me = lax.axis_index("sp")
    col = lax.axis_index("tp")
    partner = col + 1 - 2 * lax.rem(col, 2)
    far = [lax.rem(col + 2 * s, tp) for s in range(1, tp // 2)]
    barrier, greeted = greet(n, me, [partner] + far)
    pl.semaphore_wait(barrier, greeted)
    exchange(n, me, sums_ref, back, ssem, rsem, lsem)
    tokens = d_ref.shape[0]
    quarter = back.shape[2]
    start = pl.multiple_of(col * quarter, quarter)
    places = lax.broadcasted_iota(jnp.int32, (cap, tokens), 0)
    picked = jnp.zeros((tokens, quarter), jnp.float32)
    for e in range(n):
        here = jnp.zeros((cap, tokens), jnp.float32)
        for j in range(2):
            here = here + (slot_ref[j : j + 1, :] - e * cap == places).astype(jnp.float32)
        picked = picked + mm(here.astype(jnp.bfloat16), back[e], TN)
    own = d_ref[:, pl.ds(start, quarter)].astype(jnp.float32)
    gathered_ref[col] = (own + picked).astype(jnp.bfloat16)

    def send(block, slot, target):
        return pltpu.make_async_remote_copy(
            src_ref=gathered_ref.at[block],
            dst_ref=gathered_ref.at[block],
            send_sem=tsend.at[slot],
            recv_sem=trecv.at[slot],
            device_id={"tp": target},
            device_id_type=MESH,
        )

    across = [send(col, s + 1, far[s]) for s in range(len(far))]
    beside = send(col, 0, partner)
    for copy in across:
        copy.start()
    beside.start()
    passed = []
    for s in range(len(far)):
        across[s].wait_recv()
        block = lax.rem(col - 2 * (s + 1) + tp, tp)
        passed.append(send(block, tp // 2 + s, partner))
        passed[s].start()
    for copy in across:
        copy.wait_send()
    beside.wait()
    for copy in passed:
        copy.wait()


def state_copies(n, me, step, send_ref, recv_ref, send_sem, recv_sem):
    return [
        pltpu.make_async_remote_copy(
            src_ref=send_ref,
            dst_ref=recv_ref.at[k - 1],
            send_sem=send_sem.at[k - 1],
            recv_sem=recv_sem.at[k - 1],
            device_id={"sp": lax.rem(me + step * k + n, n)},
            device_id_type=MESH,
        )
        for k in range(1, n)
    ]


def collect(n, me, step, copies, recv_ref, total, width):
    total[...] = jnp.zeros_like(total)
    for k in range(n - 1, 0, -1):
        copies[k - 1].wait()
        source = me - step * k
        reached = jnp.logical_and(source >= 0, source < n)

        @pl.when(reached)
        def _():
            factor = recv_ref[k - 1, width : width + 1, :].astype(jnp.float32)
            total[...] = total[...] * factor + recv_ref[k - 1, :width, :].astype(jnp.float32)


def forward_kernel(
    n, scale, q_ref, k_ref, v_ref, g_ref, mixed_ref, states_ref, kept, total, send, recv, ssem, rsem
):
    me = lax.axis_index("sp")
    barrier, greeted = greet(n, me)
    length, width = v_ref.shape
    blocks = length // BLK
    causal = triangle(True)
    local = jnp.zeros(total.shape, jnp.float32)
    ahead = jnp.zeros((1, q_ref.shape[1]), jnp.float32)
    befores = []
    for b in range(blocks):
        rows = pl.ds(b * BLK, BLK)
        cumulative, _, ending = decays(g_ref, rows)
        kept[b] = local
        befores.append(ahead)
        faded = (k_ref[rows, :].astype(jnp.float32) * jnp.exp(ending - cumulative)).astype(
            jnp.bfloat16
        )
        local = local * jnp.exp(ending) + mm(v_ref[rows, :], faded, TN)
        ahead = ahead + ending
    send[:width, :] = local.astype(jnp.bfloat16)
    send[width:, :] = jnp.broadcast_to(jnp.exp(ahead), (16, ahead.shape[1])).astype(jnp.bfloat16)
    pl.semaphore_wait(barrier, greeted)
    copies = state_copies(n, me, 1, send, recv, ssem, rsem)
    for copy in copies:
        copy.start()
    inner = []
    scaled = []
    for b in range(blocks):
        rows = pl.ds(b * BLK, BLK)
        cumulative, middle, _ = decays(g_ref, rows)
        query = q_ref[rows, :].astype(jnp.float32) * scale
        key = k_ref[rows, :].astype(jnp.float32)
        lifted_q = (query * jnp.exp(cumulative - middle)).astype(jnp.bfloat16)
        lifted_k = (key * jnp.exp(middle - cumulative)).astype(jnp.bfloat16)
        scores = jnp.where(causal, mm(lifted_q, lifted_k, NT), 0.0).astype(jnp.bfloat16)
        inner.append(mm(scores, v_ref[rows, :], NN))
        scaled.append((query * jnp.exp(cumulative)).astype(jnp.bfloat16))
    collect(n, me, 1, copies, recv, total, width)
    for b in range(blocks):
        rows = pl.ds(b * BLK, BLK)
        state = (kept[b] + total[...] * jnp.exp(befores[b])).astype(jnp.bfloat16)
        states_ref[b] = state
        mixed_ref[rows, :] = (inner[b] + mm(scaled[b], state, NT)).astype(jnp.bfloat16)


def backward_kernel(
    n,
    scale,
    q_ref,
    k_ref,
    v_ref,
    g_ref,
    grad_ref,
    w_ref,
    mixed_ref,
    states_ref,
    gq_ref,
    gk_ref,
    gv_ref,
    gg_ref,
    proj_ref,
    kept,
    total,
    send,
    recv,
    ssem,
    rsem,
    d_ref,
    part,
    pair_in,
    pair,
    parts_in,
    psend,
    precv,
):
    me = lax.axis_index("sp")
    barrier, greeted = greet(n, me)
    length, width = v_ref.shape
    blocks = length // BLK
    causal = triangle(True)
    local = jnp.zeros(total.shape, jnp.float32)
    pieces, _, quarter = grad_ref.shape
    d_mixed = jnp.zeros((length, width), jnp.float32)
    for p in range(pieces):
        d_mixed = d_mixed + mm(grad_ref[p], w_ref[p * quarter : (p + 1) * quarter, :], NN)
    d_ref[...] = d_mixed.astype(jnp.bfloat16)
    after = jnp.zeros((1, q_ref.shape[1]), jnp.float32)
    afters = [None] * blocks
    for b in reversed(range(blocks)):
        rows = pl.ds(b * BLK, BLK)
        cumulative, _, ending = decays(g_ref, rows)
        kept[b] = local
        afters[b] = after
        query = q_ref[rows, :].astype(jnp.float32) * scale
        scaled = (query * jnp.exp(cumulative)).astype(jnp.bfloat16)
        local = local * jnp.exp(ending) + mm(d_ref[rows, :], scaled, TN)
        after = after + ending
    send[:width, :] = local.astype(jnp.bfloat16)
    send[width:, :] = jnp.broadcast_to(jnp.exp(after), (16, after.shape[1])).astype(jnp.bfloat16)
    pl.semaphore_wait(barrier, greeted)
    copies = state_copies(n, me, -1, send, recv, ssem, rsem)
    for copy in copies:
        copy.start()
    half, share = part.shape[1:3]
    per = quarter // share
    for p in range(pieces):
        product = mm(grad_ref[p], mixed_ref[...], TN).astype(jnp.bfloat16)
        for i in range(per):
            at = p * per + i
            part[at % 2, at // 2] = product[i * share : (i + 1) * share, :]
    parity = lax.rem(me, 2)
    mine = me // 2
    pairing = pltpu.make_async_remote_copy(
        src_ref=part.at[1 - parity],
        dst_ref=pair_in,
        send_sem=psend.at[0],
        recv_sem=precv.at[0],
        device_id={"sp": me + 1 - 2 * parity},
        device_id_type=MESH,
    )
    pairing.start()
    change = []
    key_part = []
    for b in range(blocks):
        rows = pl.ds(b * BLK, BLK)
        cumulative, middle, _ = decays(g_ref, rows)
        query = q_ref[rows, :].astype(jnp.float32) * scale
        key = k_ref[rows, :].astype(jnp.float32)
        value = v_ref[rows, :]
        d_out = d_ref[rows, :]
        rise, fall = jnp.exp(cumulative - middle), jnp.exp(middle - cumulative)
        lifted_q = (query * rise).astype(jnp.bfloat16)
        lifted_k = (key * fall).astype(jnp.bfloat16)
        scores = jnp.where(causal, mm(lifted_q, lifted_k, NT), 0.0).astype(jnp.bfloat16)
        d_scores = jnp.where(causal, mm(d_out, value, NT), 0.0).astype(jnp.bfloat16)
        d_lifted_q = mm(d_scores, lifted_k, NN)
        d_lifted_k = mm(d_scores, lifted_q, TN)
        grown = jnp.exp(cumulative)
        d_carried = mm(d_out, states_ref[b], NN) * grown
        gq_ref[rows, :] = ((d_lifted_q * rise + d_carried) * scale).astype(jnp.bfloat16)
        change.append(
            lifted_q.astype(jnp.float32) * d_lifted_q
            - lifted_k.astype(jnp.float32) * d_lifted_k
            + query * d_carried
        )
        key_part.append(d_lifted_k * fall)
        gg_ref[rows, :] = change[b]
        gv_ref[rows, :] = mm(scores, d_out, TN).astype(gv_ref.dtype)
    pairing.wait()
    for i in range(half):
        pair[i] = (part[parity, i].astype(jnp.float32) + pair_in[i].astype(jnp.float32)).astype(
            jnp.bfloat16
        )
    collect(n, me, -1, copies, recv, total, width)
    shares = []
    for s in range(1, half):
        other = lax.rem(mine + s, half)
        shares.append(
            pltpu.make_async_remote_copy(
                src_ref=pair.at[other],
                dst_ref=parts_in.at[s - 1],
                send_sem=psend.at[s],
                recv_sem=precv.at[s],
                device_id={"sp": 2 * other + parity},
                device_id_type=MESH,
            )
        )
        shares[-1].start()
    for b in range(blocks):
        rows = pl.ds(b * BLK, BLK)
        cumulative, _, ending = decays(g_ref, rows)
        d_state = kept[b] + total[...] * jnp.exp(afters[b])
        d_rounded = d_state.astype(jnp.bfloat16)
        key = k_ref[rows, :].astype(jnp.float32)
        fade = jnp.exp(ending - cumulative)
        faded = key * fade
        d_faded = mm(v_ref[rows, :], d_rounded, NN)
        gk_ref[rows, :] = (key_part[b] + d_faded * fade).astype(jnp.bfloat16)
        gv_ref[rows, :] = gv_ref[rows, :] + mm(faded.astype(jnp.bfloat16), d_rounded, NT)
        moved = faded * d_faded
        at_end = jnp.sum(moved, axis=0, keepdims=True) + jnp.exp(ending) * jnp.sum(
            states_ref[b].astype(jnp.float32) * d_state, axis=0, keepdims=True
        )
        gg_ref[rows, :] = block_sums(triangle(False), gg_ref[rows, :] - moved) + at_end
    summed = pair[mine].astype(jnp.float32)
    for s in range(1, half):
        shares[s - 1].wait()
        summed = summed + parts_in[s - 1].astype(jnp.float32)
    proj_ref[...] = summed


def exchange_scratch(n, blocks, width, channels):
    return [
        pltpu.VMEM((blocks, width, channels), jnp.float32),
        pltpu.VMEM((width, channels), jnp.float32),
        pltpu.VMEM((width + 16, channels), jnp.bfloat16),
        pltpu.VMEM((n - 1, width + 16, channels), jnp.bfloat16),
        pltpu.SemaphoreType.DMA((n - 1,)),
        pltpu.SemaphoreType.DMA((n - 1,)),
    ]


def in_vmem(count):
    return [pl.BlockSpec(memory_space=pltpu.VMEM)] * count


def mixer_forward(q, k, v, g, scale):
    n = lax.axis_size("sp")
    length, channels = q.shape
    width = v.shape[1]
    blocks = length // BLK
    return pl.pallas_call(
        functools.partial(forward_kernel, n, scale),
        out_shape=(
            jax.ShapeDtypeStruct((length, width), jnp.bfloat16),
            jax.ShapeDtypeStruct((blocks, width, channels), jnp.bfloat16),
        ),
        in_specs=in_vmem(4),
        out_specs=tuple(in_vmem(2)),
        scratch_shapes=exchange_scratch(n, blocks, width, channels),
        compiler_params=pltpu.CompilerParams(
            collective_id=1, has_side_effects=True, vmem_limit_bytes=16 * 1024 * 1024
        ),
        cost_estimate=pl.CostEstimate(
            flops=4_000_000_000, bytes_accessed=4 * length * width, transcendentals=0
        ),
        name="mixer_forward",
    )(q, k, v, g)


def mixer_backward(q, k, v, g, gathered, w_out, mixed, states, scale):
    n = lax.axis_size("sp")
    length, channels = q.shape
    width = v.shape[1]
    blocks = length // BLK
    share = w_out.shape[0] // n
    return pl.pallas_call(
        functools.partial(backward_kernel, n, scale),
        out_shape=(
            jax.ShapeDtypeStruct((length, channels), jnp.bfloat16),
            jax.ShapeDtypeStruct((length, channels), jnp.bfloat16),
            jax.ShapeDtypeStruct((length, width), jnp.float32),
            jax.ShapeDtypeStruct((length, channels), jnp.float32),
            jax.ShapeDtypeStruct((share, width), jnp.float32),
        ),
        in_specs=in_vmem(8),
        out_specs=tuple(in_vmem(5)),
        scratch_shapes=exchange_scratch(n, blocks, width, channels)
        + [
            pltpu.VMEM((length, width), jnp.bfloat16),
            pltpu.VMEM((2, n // 2, share, width), jnp.bfloat16),
            pltpu.VMEM((n // 2, share, width), jnp.bfloat16),
            pltpu.VMEM((n // 2, share, width), jnp.bfloat16),
            pltpu.VMEM((n // 2 - 1, share, width), jnp.bfloat16),
            pltpu.SemaphoreType.DMA((n // 2,)),
            pltpu.SemaphoreType.DMA((n // 2,)),
        ],
        compiler_params=pltpu.CompilerParams(
            collective_id=2, has_side_effects=True, vmem_limit_bytes=24 * 1024 * 1024
        ),
        cost_estimate=pl.CostEstimate(
            flops=8_000_000_000, bytes_accessed=4 * length * width, transcendentals=0
        ),
        name="mixer_backward",
    )(q, k, v, g, gathered, w_out, mixed, states)


def route_out(d_out, route_expert, route_weight, capacity):
    n, tp = lax.axis_size("sp"), lax.axis_size("tp")
    tokens, model_width = d_out.shape
    quarter = model_width // tp
    return pl.pallas_call(
        functools.partial(route_kernel, n, tp, capacity),
        out_shape=(
            jax.ShapeDtypeStruct((n, capacity, model_width), jnp.bfloat16),
            jax.ShapeDtypeStruct((2, tokens), jnp.int32),
        ),
        in_specs=in_vmem(3),
        out_specs=tuple(in_vmem(2)),
        scratch_shapes=[
            pltpu.VMEM((n, capacity, quarter), jnp.bfloat16),
            pltpu.SemaphoreType.DMA((n - 1,)),
            pltpu.SemaphoreType.DMA((n - 1,)),
            pltpu.SemaphoreType.DMA,
            pltpu.SemaphoreType.DMA((n, tp)),
            pltpu.SemaphoreType.DMA((n, tp)),
        ],
        compiler_params=pltpu.CompilerParams(
            collective_id=3, has_side_effects=True, vmem_limit_bytes=24 * 1024 * 1024
        ),
        cost_estimate=pl.CostEstimate(
            flops=8_000_000_000, bytes_accessed=4 * tokens * quarter, transcendentals=0
        ),
        name="route_out",
    )(d_out, route_expert.T, route_weight)


def route_back(summed, slots, d_out):
    n, tp = lax.axis_size("sp"), lax.axis_size("tp")
    capacity, quarter = summed.shape[1:]
    tokens = d_out.shape[0]
    return pl.pallas_call(
        functools.partial(return_kernel, n, tp, capacity),
        out_shape=jax.ShapeDtypeStruct((tp, tokens, quarter), jnp.bfloat16),
        in_specs=in_vmem(3),
        out_specs=in_vmem(1)[0],
        scratch_shapes=[
            pltpu.VMEM((n, capacity, quarter), jnp.bfloat16),
            pltpu.SemaphoreType.DMA((n - 1,)),
            pltpu.SemaphoreType.DMA((n - 1,)),
            pltpu.SemaphoreType.DMA,
            pltpu.SemaphoreType.DMA((tp,)),
            pltpu.SemaphoreType.DMA((tp,)),
        ],
        compiler_params=pltpu.CompilerParams(
            collective_id=4, has_side_effects=True, vmem_limit_bytes=24 * 1024 * 1024
        ),
        cost_estimate=pl.CostEstimate(
            flops=8_000_000_000, bytes_accessed=4 * tokens * quarter, transcendentals=0
        ),
        name="route_back",
    )(summed, slots, d_out)


def expert_pass(rows_in, routed_rows, gate_w, up_w, down_w):
    gate_pre = jnp.dot(rows_in, gate_w, preferred_element_type=jnp.float32)
    up_pre = jnp.dot(rows_in, up_w, preferred_element_type=jnp.float32)
    sigmoid_gate = jax.nn.sigmoid(gate_pre)
    active = gate_pre * sigmoid_gate
    hidden = (active * up_pre).astype(jnp.bfloat16)
    d_hidden = lax.dot_general(
        routed_rows, down_w, (((1,), (1,)), ((), ())), preferred_element_type=jnp.float32
    )
    d_gate = (d_hidden * up_pre * sigmoid_gate * (1.0 + gate_pre * (1.0 - sigmoid_gate))).astype(
        jnp.bfloat16
    )
    d_up = (d_hidden * active).astype(jnp.bfloat16)
    rows_first = (((0,), (0,)), ((), ()))
    grad_gate = lax.dot_general(
        rows_in, d_gate, rows_first, preferred_element_type=jnp.float32
    ).astype(jnp.bfloat16)
    grad_up = lax.dot_general(rows_in, d_up, rows_first, preferred_element_type=jnp.float32).astype(
        jnp.bfloat16
    )
    grad_down = lax.dot_general(
        hidden, routed_rows, rows_first, preferred_element_type=jnp.float32
    ).astype(jnp.bfloat16)
    return (grad_gate, grad_up, grad_down, d_gate, d_up)


def local(
    d_out,
    route_expert,
    route_weight,
    expert_inputs,
    w_gate,
    w_up,
    w_down,
    w_out,
    queries,
    keys,
    values,
    log_decay,
):
    model_width = d_out.shape[1]
    experts = lax.axis_size("sp")
    capacity = expert_inputs.shape[1] // experts
    quarter = model_width // lax.axis_size("tp")
    routed, slots = route_out(d_out, route_expert, route_weight, capacity)
    routed = routed.reshape(experts * capacity, model_width)
    rows_in = expert_inputs[0]
    gate_w = w_gate[0]
    up_w = w_up[0]
    grad_gate, grad_up, grad_down, d_gate, d_up = expert_pass(
        rows_in, routed, gate_w, up_w, w_down[0]
    )
    partial_terms = lax.dot_general(
        d_gate, gate_w, (((1,), (1,)), ((), ())), preferred_element_type=jnp.float32
    )
    partial_terms = partial_terms + lax.dot_general(
        d_up, up_w, (((1,), (1,)), ((), ())), preferred_element_type=jnp.float32
    )
    rounded = lax.optimization_barrier(partial_terms.astype(jnp.bfloat16)).astype(jnp.float32)
    summed = lax.psum_scatter(rounded.astype(jnp.bfloat16), "tp", scatter_dimension=1, tiled=True)
    scale_q = queries.shape[2] ** (-0.5)
    q, k, v, g = queries[:, 0], keys[:, 0], values[:, 0], log_decay[:, 0]
    mixed, states = mixer_forward(q, k, v, g, scale_q)
    summed, mixed, grad_gate, grad_up, grad_down = lax.optimization_barrier(
        (summed, mixed, grad_gate, grad_up, grad_down)
    )
    gathered = route_back(summed.reshape(experts, capacity, quarter), slots, d_out)
    grad_q, grad_k, grad_v, grad_g, grad_proj = mixer_backward(
        q, k, v, g, gathered, w_out, mixed, states, scale_q
    )
    return (
        grad_gate[None],
        grad_up[None],
        grad_down[None],
        grad_proj,
        grad_q[:, None],
        grad_k[:, None],
        grad_v.astype(jnp.bfloat16)[:, None],
        grad_g[:, None],
    )


def paired(me, offset):
    other = me
    bit = 1
    while bit <= offset:
        if offset & bit:
            other = other + bit - 2 * bit * lax.rem(me // bit, 2)
        bit *= 2
    return other


def prefix_copy(n, me, step, distance, index, send, recv, ssem, rsem):
    return pltpu.make_async_remote_copy(
        src_ref=send.at[index],
        dst_ref=recv.at[index],
        send_sem=ssem.at[index],
        recv_sem=rsem.at[index],
        device_id={"sp": lax.rem(me + step * distance + n, n)},
        device_id_type=MESH,
    )


def prefix_send(n, me, step, distance, index, local, ahead, scan, send, recv, ssem, rsem):
    width = local.shape[0]
    total, reach = scan
    decay = reach[0:1, :] * ahead[0:1, :]
    send[index, :width, :] = (total[...] * ahead[0:1, :] + local[...]).astype(jnp.bfloat16)
    send[index, width:, :] = jnp.broadcast_to(decay, (16, decay.shape[1])).astype(jnp.bfloat16)
    target = me + step * distance

    @pl.when(jnp.logical_and(target >= 0, target < n))
    def _():
        prefix_copy(n, me, step, distance, index, send, recv, ssem, rsem).start()


def prefix_take(n, me, step, distance, index, scan, send, recv, ssem, rsem):
    total, reach = scan
    width = total.shape[0]
    source = me - step * distance
    target = me + step * distance
    copy = prefix_copy(n, me, step, distance, index, send, recv, ssem, rsem)

    @pl.when(jnp.logical_and(target >= 0, target < n))
    def _():
        copy.wait_send()

    @pl.when(jnp.logical_and(source >= 0, source < n))
    def _():
        copy.wait_recv()
        total[...] = total[...] + recv[index, :width, :].astype(jnp.float32) * reach[0:1, :]
        reach[...] = reach[...] * recv[index, width : width + 1, :].astype(jnp.float32)


def distances(n):
    found = []
    step = 1
    while step < n:
        found.append(step)
        step *= 2
    return found


def expert_kernel(
    n,
    cap,
    scale,
    d_hbm,
    expert_ref,
    weight_ref,
    x_hbm,
    wg_hbm,
    wu_hbm,
    wd_hbm,
    q_ref,
    k_ref,
    v_ref,
    g_ref,
    w_hbm,
    grad_gate,
    grad_up,
    grad_down,
    grad_proj,
    grad_q,
    grad_k,
    grad_v,
    grad_g,
    wg_ref,
    wu_ref,
    wd_ref,
    proj_ref,
    gq_ref,
    gk_ref,
    gv_ref,
    gg_ref,
    gathered,
    mixed_ref,
    states_ref,
    d_ref,
    x_ref,
    routed,
    onehot,
    outbox,
    outbox_near,
    slope,
    active,
    hidden,
    d_gate,
    d_up,
    part,
    pair_in,
    far_out,
    far_in,
    sums,
    back,
    picked,
    turned,
    cum,
    kept,
    befores,
    inner,
    scaled,
    lifted_q,
    lifted_k,
    scores_ref,
    d_round,
    key_part,
    proj_out,
    proj_pair,
    proj_mine,
    proj_in,
    w_ref,
    mix_local,
    mix_ahead,
    mix_total,
    mix_reach,
    mix_send,
    mix_recv,
    lsem,
    osem,
    rs,
    rr,
    fs,
    fr,
    ps,
    pr,
    qs,
    qr,
    ds,
    dr,
    xs,
    xr,
    bs,
    br,
    ms,
    mr,
    gs,
    gr,
    ys,
    yr,
    zs,
    zr,
):
    me = lax.axis_index("sp")
    col = lax.axis_index("tp")
    core = lax.rem(col, 2)
    side = col // 2
    partner = col + 1 - 2 * core
    far = lax.rem(col + 2, 4)
    chunks = n // 2
    rows2 = 2 * cap
    tokens = d_ref.shape[0]
    model = d_ref.shape[1]
    quarter = model // 4
    half = model // 2
    near = 3

    barrier, greeted = greet(n, me, [partner, far])

    def chunk_rows(z):
        return pl.ds(z * rows2, rows2)

    def block_rows(m):
        return pl.ds(m * cap, cap)

    def columns(q):
        return pl.ds(pl.multiple_of(q * quarter, quarter), quarter)

    order = [0] + list(range(chunks - 1, 0, -1))
    loads = {}

    def load(name, source, target, index):
        loads[name] = pltpu.make_async_copy(source, target, lsem.at[index])
        loads[name].start()

    load("d", d_hbm, d_ref, 0)
    load("wg", wg_hbm, wg_ref, 1)

    def load_rows(z):
        for m in (2 * z, 2 * z + 1):
            first = pl.multiple_of(paired(me, m) * cap, cap)
            load(("x", m), x_hbm.at[pl.ds(first, cap), :], x_ref.at[block_rows(m), :], 4 + m)

    load_rows(0)
    load("wu", wu_hbm, wu_ref, 2)
    load("wd", wd_hbm, wd_ref, 3)
    for z in order[1:]:
        load_rows(z)
    load("w", w_hbm, w_ref, 4 + n)

    kinds = lax.broadcasted_iota(jnp.int32, (n, tokens), 0)
    named = [(kinds == expert_ref[j : j + 1, :]).astype(jnp.float32) for j in range(2)]
    earlier = lax.broadcasted_iota(jnp.int32, (tokens, tokens), 0) < lax.broadcasted_iota(
        jnp.int32, (tokens, tokens), 1
    )
    before = mm((named[0] + named[1]).astype(jnp.bfloat16), earlier.astype(jnp.bfloat16), NN)
    slots = []
    for j in range(2):
        rank = jnp.sum(before * named[j], axis=0, keepdims=True).astype(jnp.int32)
        slots.append(expert_ref[j : j + 1, :] * cap + rank)
    places = lax.broadcasted_iota(jnp.int32, (cap, tokens), 0)

    def routed_rows(m, chosen):
        first = paired(me, m) * cap
        hits = [(slots[j] - first == places).astype(jnp.float32) for j in range(2)]
        both = (hits[0] + hits[1]).astype(jnp.bfloat16)
        onehot[block_rows(m), :] = both
        weight = jnp.sum(
            hits[0] * weight_ref[0:1, :] + hits[1] * weight_ref[1:2, :], axis=1, keepdims=True
        )
        return (mm(both, chosen, NN) * weight).astype(jnp.bfloat16)

    def route(m):
        if m <= near:
            source = outbox_near.at[block_rows(m - 1), :]
            target = routed.at[block_rows(m), pl.ds(pl.multiple_of(core * half, half), half)]
        else:
            source = outbox.at[block_rows(m - near - 1), :]
            target = routed.at[block_rows(m), columns(col)]
        return pltpu.make_async_remote_copy(
            src_ref=source,
            dst_ref=target,
            send_sem=rs.at[m],
            recv_sem=rr.at[m],
            device_id={"sp": paired(me, m)},
            device_id_type=MESH,
        )

    def pass_on(m, what, target, send_sem, recv_sem):
        if m <= near:
            piece = routed.at[block_rows(m), pl.ds(pl.multiple_of(what * half, half), half)]
        else:
            piece = routed.at[block_rows(m), columns(what)]
        return pltpu.make_async_remote_copy(
            src_ref=piece,
            dst_ref=piece,
            send_sem=send_sem.at[m],
            recv_sem=recv_sem.at[m],
            device_id={"tp": target},
            device_id_type=MESH,
        )

    sent = []
    loads["d"].wait()
    sends = []
    for z in order[1:]:
        sends += [2 * z, 2 * z + 1]
    sends.insert(1, 1)
    greeting = True
    for m in sends:
        if m <= near:
            outbox_near[block_rows(m - 1), :] = routed_rows(
                m, d_ref[:, pl.ds(pl.multiple_of(core * half, half), half)]
            )
        else:
            outbox[block_rows(m - near - 1), :] = routed_rows(m, d_ref[:, columns(col)])
        if greeting:
            pl.semaphore_wait(barrier, greeted)
            greeting = False
        sent.append(route(m))
        sent[-1].start()
    routed[block_rows(0), :] = routed_rows(0, d_ref[...])

    crossed, beside, relayed = {}, {}, {}

    def arrive(m):
        route(m).wait_recv()
        if m <= near:
            beside[m] = pass_on(m, core, partner, ps, pr)
            beside[m].start()
            return
        crossed[m] = pass_on(m, col, far, fs, fr)
        crossed[m].start()
        beside[m] = pass_on(m, col, partner, ps, pr)
        beside[m].start()

    def relay(m):
        if m <= near:
            return
        crossed[m].wait_recv()
        relayed[m] = pass_on(m, far, partner, qs, qr)
        relayed[m].start()

    def complete(m):
        beside[m].wait_recv()
        if m > near:
            relayed[m].wait_recv()

    def gates(z):
        rows = chunk_rows(z)
        held = order.index(z) % 2
        loads[("x", 2 * z)].wait()
        loads[("x", 2 * z + 1)].wait()
        if z == 0:
            loads["wg"].wait()
        gate = mm(x_ref[rows, :], wg_ref[...], NT)
        if z == 0:
            loads["wu"].wait()
        up = mm(x_ref[rows, :], wu_ref[...], NT)
        sigmoid = jax.nn.sigmoid(gate)
        silu = gate * sigmoid
        hidden[rows, :] = (silu * up).astype(jnp.bfloat16)
        active[held] = silu
        slope[held] = up * sigmoid * (1.0 + gate * (1.0 - sigmoid))

    halves = {}

    def experts(z):
        rows = chunk_rows(z)
        if z == 0:
            loads["wd"].wait()
        d_hidden = mm(routed[rows, :], wd_ref[...], NT)
        held = order.index(z) % 2
        d_gate[rows, :] = (d_hidden * slope[held]).astype(jnp.bfloat16)
        d_up[rows, :] = (d_hidden * active[held]).astype(jnp.bfloat16)
        for whose in (1 - core, core):
            for i in range(2):
                across = 1 - side if i == 0 else side
                cut = columns(2 * across + whose)
                term = mm(d_gate[rows, :], wg_ref[:, cut], NN) + mm(
                    d_up[rows, :], wu_ref[:, cut], NN
                )
                part[rows, cut] = term.astype(jnp.bfloat16)
            if (z, 0) in halves:
                continue
            for i in range(2):
                across = 1 - side if i == 0 else side
                halves[(z, i)] = pltpu.make_async_remote_copy(
                    src_ref=part.at[rows, columns(2 * across + 1 - core)],
                    dst_ref=pair_in.at[i, rows, :],
                    send_sem=ds.at[z, i],
                    recv_sem=dr.at[z, i],
                    device_id={"tp": partner},
                    device_id_type=MESH,
                )
                halves[(z, i)].start()

    over = {}

    def reduce_near(z):
        rows = chunk_rows(z)
        halves[(z, 0)].wait_recv()
        far_out[rows, :] = (
            part[rows, columns(far)].astype(jnp.float32)
            + pair_in[0, rows, :].astype(jnp.float32)
        ).astype(jnp.bfloat16)
        over[z] = pltpu.make_async_remote_copy(
            src_ref=far_out.at[rows, :],
            dst_ref=far_in.at[rows, :],
            send_sem=xs.at[z],
            recv_sem=xr.at[z],
            device_id={"tp": far},
            device_id_type=MESH,
        )
        over[z].start()

    returned = {}

    def reduce_far(z):
        rows = chunk_rows(z)
        halves[(z, 1)].wait_recv()
        over[z].wait_recv()
        sums[rows, :] = (
            part[rows, columns(col)].astype(jnp.float32)
            + pair_in[1, rows, :].astype(jnp.float32)
            + far_in[rows, :].astype(jnp.float32)
        ).astype(jnp.bfloat16)
        for m in (2 * z, 2 * z + 1):
            if m == 0:
                back[block_rows(0), :] = sums[block_rows(0), :]
                continue
            returned[m] = pltpu.make_async_remote_copy(
                src_ref=sums.at[block_rows(m), :],
                dst_ref=back.at[block_rows(m), :],
                send_sem=bs.at[m],
                recv_sem=br.at[m],
                device_id={"sp": paired(me, m)},
                device_id_type=MESH,
            )
            returned[m].start()

    def pick(z):
        rows = chunk_rows(z)
        for m in (2 * z, 2 * z + 1):
            if m > 0:
                returned[m].wait_recv()
        found = mm(onehot[rows, :], back[rows, :], TN)
        picked[...] = found if z == 0 else picked[...] + found

    stored = []

    def store(source, target):
        stored.append(pltpu.make_async_copy(source, target, osem.at[len(stored)]))
        stored[-1].start()

    def weight_grad(lhs, rhs, out, target):
        turned[...] = lhs[...].T

        def piece(i, carry):
            cut = columns(i)
            out[:, cut] = mm(turned[...], rhs[:, cut], NN).astype(jnp.bfloat16)
            return carry

        lax.fori_loop(0, 4, piece, 0)
        store(out, target)

    blocks = tokens // BLK
    causal = triangle(True)
    width = v_ref.shape[1]
    scan = (mix_total, mix_reach)
    reach = distances(n)
    rounds = len(reach)

    def scan_from(local, ahead):
        mix_local[...] = local
        mix_ahead[...] = jnp.broadcast_to(jnp.exp(ahead), mix_ahead.shape)
        mix_total[...] = jnp.zeros(mix_total.shape, jnp.float32)
        mix_reach[...] = jnp.ones(mix_reach.shape, jnp.float32)

    def mixer_states():
        local = jnp.zeros(mix_total.shape, jnp.float32)
        ahead = jnp.zeros((1, q_ref.shape[1]), jnp.float32)
        for b in range(blocks):
            rows = pl.ds(b * BLK, BLK)
            cumulative, _, ending = decays(g_ref, rows)
            cum[rows, :] = cumulative
            kept[b] = local
            befores[b : b + 1, :] = jnp.exp(ahead)
            faded = (k_ref[rows, :].astype(jnp.float32) * jnp.exp(ending - cumulative)).astype(
                jnp.bfloat16
            )
            local = local * jnp.exp(ending) + mm(v_ref[rows, :], faded, TN)
            ahead = ahead + ending
        scan_from(local, ahead)

    def mixer_send(step, index):
        at = index if step > 0 else rounds + index
        distance = reach[index]
        prefix_send(
            n, me, step, distance, at, mix_local, mix_ahead, scan, mix_send, mix_recv, ms, mr
        )

    def mixer_take(step, index):
        at = index if step > 0 else rounds + index
        prefix_take(n, me, step, reach[index], at, scan, mix_send, mix_recv, ms, mr)

    def mixer_inner():
        for b in range(blocks):
            rows = pl.ds(b * BLK, BLK)
            cumulative = cum[rows, :]
            middle = cumulative[BLK // 2 - 1 : BLK // 2, :]
            query = q_ref[rows, :].astype(jnp.float32) * scale
            key = k_ref[rows, :].astype(jnp.float32)
            up_q = (query * jnp.exp(cumulative - middle)).astype(jnp.bfloat16)
            up_k = (key * jnp.exp(middle - cumulative)).astype(jnp.bfloat16)
            scores = jnp.where(causal, mm(up_q, up_k, NT), 0.0).astype(jnp.bfloat16)
            lifted_q[rows, :] = up_q
            lifted_k[rows, :] = up_k
            scores_ref[rows, :] = scores
            inner[rows, :] = mm(scores, v_ref[rows, :], NN)
            scaled[rows, :] = (query * jnp.exp(cumulative)).astype(jnp.bfloat16)

    def mixer_finish():
        for b in range(blocks):
            rows = pl.ds(b * BLK, BLK)
            state = (kept[b] + mix_total[...] * befores[b : b + 1, :]).astype(jnp.bfloat16)
            states_ref[b] = state
            mixed_ref[rows, :] = (inner[rows, :] + mm(scaled[rows, :], state, NT)).astype(
                jnp.bfloat16
            )

    taken = [0]

    def mixer_round(step):
        if taken[0] < rounds:
            mixer_take(step, taken[0])
            taken[0] += 1
            if taken[0] < rounds:
                mixer_send(step, taken[0])

    share, turns = proj_out.shape[3], proj_out.shape[1]
    parity = lax.rem(me, 2)
    at_z = me // 2
    paired_off, handed = {}, []

    def project(j):
        q = paired(col, j)
        rows = pl.ds(pl.multiple_of(q * quarter, quarter), quarter)
        grads = gathered[j]
        term = mm(grads, w_ref[rows, :], NN)
        picked[:, :width] = term if j == 0 else picked[:, :width] + term
        product = mm(grads, mixed_ref[...], TN).astype(jnp.bfloat16)
        for i in range(turns):
            for y in range(2):
                at = 2 * i + y
                proj_out[j, i, y] = product[at * share : (at + 1) * share, :]

    def pair_up(j):
        for i in range(turns):
            paired_off[(j, i)] = pltpu.make_async_remote_copy(
                src_ref=proj_out.at[j, i, 1 - parity],
                dst_ref=proj_pair.at[j, i],
                send_sem=ys.at[j, i],
                recv_sem=yr.at[j, i],
                device_id={"sp": me + 1 - 2 * parity},
                device_id_type=MESH,
            )
            paired_off[(j, i)].start()

    def hand_over(j):
        q = paired(col, j)
        for i in range(turns):
            paired_off[(j, i)].wait_recv()
            both_rows = proj_out[j, i, parity].astype(jnp.float32) + proj_pair[j, i].astype(
                jnp.float32
            )
            proj_out[j, i, parity] = both_rows.astype(jnp.bfloat16)
            owner = q * turns + i
            away = jnp.int32(0)
            bit = 1
            while bit < chunks:
                away = away + bit * lax.rem(at_z // bit + owner // bit, 2)
                bit *= 2
            copy = pltpu.make_async_remote_copy(
                src_ref=proj_out.at[j, i, parity],
                dst_ref=proj_in.at[away],
                send_sem=zs.at[j, i],
                recv_sem=zr.at[away],
                device_id={"sp": 2 * owner + parity},
                device_id_type=MESH,
            )
            handed.append((away, copy))

            @pl.when(away == 0)
            def _():
                proj_mine[...] = proj_out[j, i, parity].astype(jnp.float32)

            @pl.when(away != 0)
            def _():
                copy.start()

    def project_sum():
        total = proj_mine[...]
        for z in range(1, chunks):
            pltpu.make_async_remote_copy(
                src_ref=proj_out.at[0, 0, parity],
                dst_ref=proj_in.at[z],
                send_sem=zs.at[0, 0],
                recv_sem=zr.at[z],
                device_id={"sp": paired(me, 2 * z)},
                device_id_type=MESH,
            ).wait_recv()
            total = total + proj_in[z].astype(jnp.float32)
        proj_ref[...] = total

    def back_states():
        d_round[...] = picked[:, :width].astype(jnp.bfloat16)
        local = jnp.zeros(mix_total.shape, jnp.float32)
        after = jnp.zeros((1, q_ref.shape[1]), jnp.float32)
        for b in reversed(range(blocks)):
            rows = pl.ds(b * BLK, BLK)
            ending = cum[b * BLK + BLK - 1 : b * BLK + BLK, :]
            kept[b] = local
            befores[b : b + 1, :] = jnp.exp(after)
            local = local * jnp.exp(ending) + mm(d_round[rows, :], scaled[rows, :], TN)
            after = after + ending
        scan_from(local, after)

    def back_inner():
        for b in range(blocks):
            rows = pl.ds(b * BLK, BLK)
            cumulative = cum[rows, :]
            middle = cumulative[BLK // 2 - 1 : BLK // 2, :]
            query = q_ref[rows, :].astype(jnp.float32) * scale
            d_out = d_round[rows, :]
            up_q, up_k = lifted_q[rows, :], lifted_k[rows, :]
            d_scores = jnp.where(causal, mm(d_out, v_ref[rows, :], NT), 0.0).astype(jnp.bfloat16)
            d_up_q = mm(d_scores, up_k, NN)
            d_up_k = mm(d_scores, up_q, TN)
            d_carried = mm(d_out, states_ref[b], NN) * jnp.exp(cumulative)
            gq_ref[rows, :] = (
                (d_up_q * jnp.exp(cumulative - middle) + d_carried) * scale
            ).astype(jnp.bfloat16)
            gg_ref[rows, :] = (
                up_q.astype(jnp.float32) * d_up_q
                - up_k.astype(jnp.float32) * d_up_k
                + query * d_carried
            )
            key_part[rows, :] = d_up_k * jnp.exp(middle - cumulative)
            inner[rows, :] = mm(scores_ref[rows, :], d_out, TN)

    def back_finish():
        for b in range(blocks):
            rows = pl.ds(b * BLK, BLK)
            cumulative = cum[rows, :]
            ending = cumulative[BLK - 1 : BLK, :]
            d_state = kept[b] + mix_total[...] * befores[b : b + 1, :]
            d_rounded = d_state.astype(jnp.bfloat16)
            fade = jnp.exp(ending - cumulative)
            faded = k_ref[rows, :].astype(jnp.float32) * fade
            d_faded = mm(v_ref[rows, :], d_rounded, NN)
            gk_ref[rows, :] = (key_part[rows, :] + d_faded * fade).astype(jnp.bfloat16)
            gv_ref[rows, :] = (
                inner[rows, :] + mm(faded.astype(jnp.bfloat16), d_rounded, NT)
            ).astype(jnp.bfloat16)
            moved = faded * d_faded
            at_end = jnp.sum(moved, axis=0, keepdims=True) + jnp.exp(ending) * jnp.sum(
                states_ref[b].astype(jnp.float32) * d_state, axis=0, keepdims=True
            )
            gg_ref[rows, :] = block_sums(triangle(False), gg_ref[rows, :] - moved) + at_end

    def both(step, z):
        step(2 * z)
        step(2 * z + 1)

    early = order[1:]
    gates(0)
    mixer_states()
    mixer_send(1, 0)
    arrive(1)
    gates(early[0])
    complete(1)
    experts(0)
    both(arrive, early[0])
    reduce_near(0)
    for i, z in enumerate(early):
        following = early[i + 1] if i + 1 < len(early) else None
        if i == 0:
            mixer_inner()
        if following is not None:
            gates(following)
        both(relay, z)
        both(complete, z)
        experts(z)
        if following is not None:
            both(arrive, following)
        reduce_near(z)
        if following is not None:
            mixer_round(1)
        reduce_far(order[i])
    pick(0)
    reduce_far(order[-1])
    while taken[0] < rounds:
        mixer_round(1)
    mixer_finish()
    weight_grad(hidden, routed, wd_ref, grad_down)
    for z in early:
        pick(z)
    own = d_ref[:, columns(col)].astype(jnp.float32)
    gathered[0] = (own + picked[...]).astype(jnp.bfloat16)

    def give(block, slot, target):
        return pltpu.make_async_remote_copy(
            src_ref=gathered.at[block],
            dst_ref=gathered.at[slot],
            send_sem=gs.at[slot],
            recv_sem=gr.at[slot],
            device_id={"tp": target},
            device_id_type=MESH,
        )

    given = [give(0, 1, partner), give(0, 2, far), give(2, 3, partner)]
    given[1].start()
    given[0].start()
    loads["w"].wait()
    project(0)
    pair_up(0)
    given[0].wait_recv()
    project(1)
    pair_up(1)
    weight_grad(d_gate, x_ref, wg_ref, grad_gate)
    hand_over(0)
    hand_over(1)
    weight_grad(d_up, x_ref, wu_ref, grad_up)
    given[1].wait_recv()
    given[2].start()
    project(2)
    pair_up(2)
    given[2].wait_recv()
    project(3)
    back_states()
    taken[0] = 0
    mixer_send(-1, 0)
    pair_up(3)
    back_inner()
    mixer_round(-1)
    mixer_round(-1)
    hand_over(2)
    hand_over(3)
    mixer_round(-1)
    store(gq_ref, grad_q)
    back_finish()
    store(gk_ref, grad_k)
    store(gv_ref, grad_v)
    store(gg_ref, grad_g)
    project_sum()
    store(proj_ref, grad_proj)
    for copy in stored:
        copy.wait()
    for copy in sent + given:
        copy.wait_send()
    for group in (crossed, beside, relayed, halves, over, returned, paired_off):
        for copy in group.values():
            copy.wait_send()
    for away, copy in handed:

        @pl.when(away != 0)
        def _():
            copy.wait_send()


def expert_stage(
    d_out, route_expert, route_weight, rows_in, gate_t, up_t, down, q, k, v, g, w_out, cap, scale
):
    n = lax.axis_size("sp")
    tokens, model = d_out.shape
    quarter = model // 4
    units = down.shape[0]
    slots = n * cap
    channels, width = q.shape[1], v.shape[1]
    blocks = tokens // BLK
    rounds = len(distances(n))
    share = model // n
    turns = n // 8
    bf16, f32 = jnp.bfloat16, jnp.float32
    weight_shape = jax.ShapeDtypeStruct((units, model), bf16)
    out_shape = (
        weight_shape,
        weight_shape,
        weight_shape,
        jax.ShapeDtypeStruct((share, width), f32),
        jax.ShapeDtypeStruct((tokens, channels), bf16),
        jax.ShapeDtypeStruct((tokens, channels), bf16),
        jax.ShapeDtypeStruct((tokens, width), bf16),
        jax.ShapeDtypeStruct((tokens, channels), f32),
    )
    anywhere = pl.BlockSpec(memory_space=pl.ANY)
    local = pl.BlockSpec(memory_space=pltpu.VMEM)
    dma = pltpu.SemaphoreType.DMA
    return pl.pallas_call(
        functools.partial(expert_kernel, n, cap, scale),
        out_shape=out_shape,
        in_specs=[anywhere, local, local] + [anywhere] * 4 + [local] * 4 + [anywhere],
        out_specs=(anywhere,) * 8,
        scratch_shapes=[pltpu.VMEM(a.shape, a.dtype) for a in out_shape]
        + [
            pltpu.VMEM((4, tokens, quarter), bf16),
            pltpu.VMEM((tokens, width), bf16),
            pltpu.VMEM((blocks, width, channels), bf16),
            pltpu.VMEM((tokens, model), bf16),
            pltpu.VMEM((slots, model), bf16),
            pltpu.VMEM((slots, model), bf16),
            pltpu.VMEM((slots, tokens), bf16),
            pltpu.VMEM((slots - 4 * cap, quarter), bf16),
            pltpu.VMEM((3 * cap, model // 2), bf16),
            pltpu.VMEM((2, 2 * cap, units), f32),
            pltpu.VMEM((2, 2 * cap, units), f32),
            pltpu.VMEM((slots, units), bf16),
            pltpu.VMEM((slots, units), bf16),
            pltpu.VMEM((slots, units), bf16),
            pltpu.VMEM((slots, model), bf16),
            pltpu.VMEM((2, slots, quarter), bf16),
            pltpu.VMEM((slots, quarter), bf16),
            pltpu.VMEM((slots, quarter), bf16),
            pltpu.VMEM((slots, quarter), bf16),
            pltpu.VMEM((slots, quarter), bf16),
            pltpu.VMEM((tokens, quarter), f32),
            pltpu.VMEM((units, slots), bf16),
            pltpu.VMEM((tokens, channels), f32),
            pltpu.VMEM((blocks, width, channels), f32),
            pltpu.VMEM((blocks, channels), f32),
            pltpu.VMEM((tokens, width), f32),
            pltpu.VMEM((tokens, channels), bf16),
            pltpu.VMEM((tokens, channels), bf16),
            pltpu.VMEM((tokens, channels), bf16),
            pltpu.VMEM((tokens, BLK), bf16),
            pltpu.VMEM((tokens, width), bf16),
            pltpu.VMEM((tokens, channels), f32),
            pltpu.VMEM((4, turns, 2, share, width), bf16),
            pltpu.VMEM((4, turns, share, width), bf16),
            pltpu.VMEM((share, width), f32),
            pltpu.VMEM((n // 2, share, width), bf16),
            pltpu.VMEM((model, width), bf16),
            pltpu.VMEM((width, channels), f32),
            pltpu.VMEM((8, channels), f32),
            pltpu.VMEM((width, channels), f32),
            pltpu.VMEM((8, channels), f32),
            pltpu.VMEM((2 * rounds, width + 16, channels), bf16),
            pltpu.VMEM((2 * rounds, width + 16, channels), bf16),
            dma((5 + n,)),
            dma((8,)),
            dma((n,)),
            dma((n,)),
            dma((n,)),
            dma((n,)),
            dma((n,)),
            dma((n,)),
            dma((n,)),
            dma((n,)),
            dma((n // 2, 2)),
            dma((n // 2, 2)),
            dma((n // 2,)),
            dma((n // 2,)),
            dma((n,)),
            dma((n,)),
            dma((2 * rounds,)),
            dma((2 * rounds,)),
            dma((4,)),
            dma((4,)),
            dma((4, turns)),
            dma((4, turns)),
            dma((4, turns)),
            dma((n // 2,)),
        ],
        compiler_params=pltpu.CompilerParams(
            collective_id=5, has_side_effects=True, vmem_limit_bytes=60 * 1024 * 1024
        ),
        cost_estimate=pl.CostEstimate(
            flops=60_000_000_000, bytes_accessed=30_000_000, transcendentals=0
        ),
        name="expert_stage",
    )(d_out, route_expert.T, route_weight.T, rows_in, gate_t, up_t, down, q, k, v, g, w_out)


def store_kernel(pieces, count, *refs):
    sources, targets, held = refs[:count], refs[count : 2 * count], refs[2 * count : 3 * count]
    isem, osem = refs[3 * count :]
    cuts = []
    for i in range(count):
        parts = pieces if i < 3 else 1
        rows = sources[i].shape[0] // parts
        cuts += [(i, pl.ds(p * rows, rows)) for p in range(parts)]
    reads = [
        pltpu.make_async_copy(sources[i].at[cut, :], held[i].at[cut, :], isem.at[at])
        for at, (i, cut) in enumerate(cuts)
    ]
    writes = [
        pltpu.make_async_copy(held[i].at[cut, :], targets[i].at[cut, :], osem.at[at])
        for at, (i, cut) in enumerate(cuts)
    ]
    for read in reads:
        read.start()
    for read, write in zip(reads, writes):
        read.wait()
        write.start()
    for write in writes:
        write.wait()


def store_out(arrays):
    count = len(arrays)
    pieces = 4 if arrays[0].shape[0] % 64 == 0 else 1
    total = 3 * pieces + count - 3
    anywhere = pl.BlockSpec(memory_space=pl.ANY)
    return pl.pallas_call(
        functools.partial(store_kernel, pieces, count),
        out_shape=tuple(jax.ShapeDtypeStruct(a.shape, a.dtype) for a in arrays),
        in_specs=[anywhere] * count,
        out_specs=(anywhere,) * count,
        scratch_shapes=[pltpu.VMEM(a.shape, a.dtype) for a in arrays]
        + [pltpu.SemaphoreType.DMA((total,)), pltpu.SemaphoreType.DMA((total,))],
        compiler_params=pltpu.CompilerParams(vmem_limit_bytes=60 * 1024 * 1024),
        name="store_out",
    )(*arrays)


def fused_local(
    d_out,
    route_expert,
    route_weight,
    expert_inputs,
    w_gate,
    w_up,
    w_down,
    w_out,
    queries,
    keys,
    values,
    log_decay,
):
    experts = lax.axis_size("sp")
    capacity = expert_inputs.shape[1] // experts
    scale_q = queries.shape[2] ** (-0.5)
    q, k, v, g = queries[:, 0], keys[:, 0], values[:, 0], log_decay[:, 0]
    results = expert_stage(
        d_out,
        route_expert,
        route_weight,
        expert_inputs[0],
        w_gate[0].T,
        w_up[0].T,
        w_down[0],
        q,
        k,
        v,
        g,
        w_out,
        capacity,
        scale_q,
    )
    grad_gate, grad_up, grad_down, grad_proj, grad_q, grad_k, grad_v, grad_g = store_out(results)
    return (
        grad_gate.T[None],
        grad_up.T[None],
        grad_down[None],
        grad_proj,
        grad_q[:, None],
        grad_k[:, None],
        grad_v[:, None],
        grad_g[:, None],
    )


def choose(*arrays):
    n, tp = lax.axis_size("sp"), lax.axis_size("tp")
    tokens, model = arrays[0].shape
    capacity = arrays[3].shape[1] // n
    power = n & (n - 1) == 0 and n % 8 == 0
    if tp == 4 and power and capacity % 16 == 0 and n * capacity <= 1536 and model % 512 == 0:
        return fused_local(*arrays)
    return local(*arrays)


def solution(mesh):
    return jax.shard_map(
        choose,
        mesh=mesh,
        in_specs=(
            P("sp", None),
            P("sp", None),
            P("sp", None),
            P("sp", None, None),
            P("sp", None, "tp"),
            P("sp", None, "tp"),
            P("sp", "tp", None),
            P(None, "tp"),
            P("sp", "tp", None),
            P("sp", "tp", None),
            P("sp", "tp", None),
            P("sp", "tp", None),
        ),
        out_specs=(
            P("sp", None, "tp"),
            P("sp", None, "tp"),
            P("sp", "tp", None),
            P("sp", "tp"),
            P("sp", "tp", None),
            P("sp", "tp", None),
            P("sp", "tp", None),
            P("sp", "tp", None),
        ),
        check_vma=False,
    )
```

profile of v0, /device:TPU:3, one launch (start us, length us, event | category | flops | bytes accessed | tf_op | source)
XLA Modules:
  0.0 131.6 jit_solution(14998237561802715180)
XLA Ops:
  0.6 123.4 %expert_stage.1 = (bf16[704,2048]{1,0:T(8,128)(2,1)}, bf16[704,2048]{1,0:T(8,128)(2,1)}, bf16[704,2048]{1,0:T(8,128)(2,1)}, f32[256,256]{1,0:T(8,128)}, bf16[512...) custom-call(bf16[512,2048]{1,0:T(8,128)(2,1)} %d_hbm.1, ...), custom_call_target="tpu_custom_call" | custom-call | flops 60000002048 | bytes 30000000 | tf_op jit(solution)/shard_map/expert_stage/pallas_call | solution.py:1431
  124.1 7.3 %store_out.1 = (bf16[704,2048]{1,0:T(8,128)(2,1)}, bf16[704,2048]{1,0:T(8,128)(2,1)}, bf16[704,2048]{1,0:T(8,128)(2,1)}, f32[256,256]{1,0:T(8,128)}, bf16[512,12...) custom-call(bf16[704,2048]{1,0:T(8,128)(2,1)} %get-tuple-element.24.refs_0_, ...), custom_call_target="tpu_custom_call" | custom-call | tf_op jit(solution)/shard_map/store_out/pallas_call | solution.py:1546
where the time goes:
time: 132 us
  Pallas kernels  131 us (99%)
    pallas_call x1, Pallas kernels, expert_stage(): pl.pallas_call(functools.partial(expert_kernel, n, cap, scale), out_shape...  123 us
    pallas_call x1, Pallas kernels, store_out(): pl.pallas_call(functools.partial(store_kernel, pieces, count), out_shape=...  7.34 us

commit v1 on v0

--- a/solution.py
+++ b/solution.py
@@ -794,6 +794,7 @@
     lifted_q,
     lifted_k,
     scores_ref,
+    d_mixed,
     d_round,
     key_part,
     proj_out,
@@ -845,6 +846,7 @@
     quarter = model // 4
     half = model // 2
     near = 3
+    cuts = [pl.ds(0, quarter // 2), pl.ds(quarter // 2, quarter // 2)]
 
     barrier, greeted = greet(n, me, [partner, far])
 
@@ -857,7 +859,7 @@
     def columns(q):
         return pl.ds(pl.multiple_of(q * quarter, quarter), quarter)
 
-    order = [0] + list(range(chunks - 1, 0, -1))
+    order = [0, chunks - 1, 1] + list(range(chunks - 2, 1, -1))
     loads = {}
 
     def load(name, source, target, index):
@@ -934,7 +936,7 @@
     sent = []
     loads["d"].wait()
     sends = []
-    for z in order[1:]:
+    for z in range(chunks - 1, 0, -1):
         sends += [2 * z, 2 * z + 1]
     sends.insert(1, 1)
     greeting = True
@@ -1028,55 +1030,64 @@
 
     over = {}
 
+    def half_of(q, h):
+        first = q * quarter + h * (quarter // 2)
+        return pl.ds(pl.multiple_of(first, quarter // 2), quarter // 2)
+
     def reduce_near(z):
         rows = chunk_rows(z)
         halves[(z, 0)].wait_recv()
-        far_out[rows, :] = (
-            part[rows, columns(far)].astype(jnp.float32)
-            + pair_in[0, rows, :].astype(jnp.float32)
-        ).astype(jnp.bfloat16)
-        over[z] = pltpu.make_async_remote_copy(
-            src_ref=far_out.at[rows, :],
-            dst_ref=far_in.at[rows, :],
-            send_sem=xs.at[z],
-            recv_sem=xr.at[z],
-            device_id={"tp": far},
-            device_id_type=MESH,
-        )
-        over[z].start()
+        for h in range(2):
+            far_out[rows, cuts[h]] = (
+                part[rows, half_of(far, h)].astype(jnp.float32)
+                + pair_in[0, rows, cuts[h]].astype(jnp.float32)
+            ).astype(jnp.bfloat16)
+            over[(z, h)] = pltpu.make_async_remote_copy(
+                src_ref=far_out.at[rows, cuts[h]],
+                dst_ref=far_in.at[rows, cuts[h]],
+                send_sem=xs.at[z, h],
+                recv_sem=xr.at[z, h],
+                device_id={"tp": far},
+                device_id_type=MESH,
+            )
+            over[(z, h)].start()
 
     returned = {}
 
     def reduce_far(z):
+        halves[(z, 1)].wait_recv()
+        for h in range(2):
+            reduce_half(z, h)
+
+    def reduce_half(z, h):
         rows = chunk_rows(z)
-        halves[(z, 1)].wait_recv()
-        over[z].wait_recv()
-        sums[rows, :] = (
-            part[rows, columns(col)].astype(jnp.float32)
-            + pair_in[1, rows, :].astype(jnp.float32)
-            + far_in[rows, :].astype(jnp.float32)
+        over[(z, h)].wait_recv()
+        sums[rows, cuts[h]] = (
+            part[rows, half_of(col, h)].astype(jnp.float32)
+            + pair_in[1, rows, cuts[h]].astype(jnp.float32)
+            + far_in[rows, cuts[h]].astype(jnp.float32)
         ).astype(jnp.bfloat16)
         for m in (2 * z, 2 * z + 1):
             if m == 0:
-                back[block_rows(0), :] = sums[block_rows(0), :]
+                back[block_rows(0), cuts[h]] = sums[block_rows(0), cuts[h]]
                 continue
-            returned[m] = pltpu.make_async_remote_copy(
-                src_ref=sums.at[block_rows(m), :],
-                dst_ref=back.at[block_rows(m), :],
-                send_sem=bs.at[m],
-                recv_sem=br.at[m],
+            returned[(m, h)] = pltpu.make_async_remote_copy(
+                src_ref=sums.at[block_rows(m), cuts[h]],
+                dst_ref=back.at[block_rows(m), cuts[h]],
+                send_sem=bs.at[m, h],
+                recv_sem=br.at[m, h],
                 device_id={"sp": paired(me, m)},
                 device_id_type=MESH,
             )
-            returned[m].start()
-
-    def pick(z):
+            returned[(m, h)].start()
+
+    def pick(z, h):
         rows = chunk_rows(z)
         for m in (2 * z, 2 * z + 1):
             if m > 0:
-                returned[m].wait_recv()
-        found = mm(onehot[rows, :], back[rows, :], TN)
-        picked[...] = found if z == 0 else picked[...] + found
+                returned[(m, h)].wait_recv()
+        found = mm(onehot[rows, :], back[rows, cuts[h]], TN)
+        picked[:, cuts[h]] = found if z == 0 else picked[:, cuts[h]] + found
 
     stored = []
 
@@ -1174,17 +1185,16 @@
     at_z = me // 2
     paired_off, handed = {}, []
 
-    def project(j):
-        q = paired(col, j)
-        rows = pl.ds(pl.multiple_of(q * quarter, quarter), quarter)
-        grads = gathered[j]
+    def project(j, h):
+        first = paired(col, j) * quarter + h * (quarter // 2)
+        rows = pl.ds(pl.multiple_of(first, quarter // 2), quarter // 2)
+        grads = gathered[j, :, cuts[h]]
         term = mm(grads, w_ref[rows, :], NN)
-        picked[:, :width] = term if j == 0 else picked[:, :width] + term
+        d_mixed[...] = term if j + h == 0 else d_mixed[...] + term
         product = mm(grads, mixed_ref[...], TN).astype(jnp.bfloat16)
-        for i in range(turns):
-            for y in range(2):
-                at = 2 * i + y
-                proj_out[j, i, y] = product[at * share : (at + 1) * share, :]
+        for t in range(turns):
+            at = h * turns + t
+            proj_out[j, at // 2, at % 2] = product[t * share : (t + 1) * share, :]
 
     def pair_up(j):
         for i in range(turns):
@@ -1245,7 +1255,7 @@
         proj_ref[...] = total
 
     def back_states():
-        d_round[...] = picked[:, :width].astype(jnp.bfloat16)
+        d_round[...] = d_mixed[...].astype(jnp.bfloat16)
         local = jnp.zeros(mix_total.shape, jnp.float32)
         after = jnp.zeros((1, q_ref.shape[1]), jnp.float32)
         for b in reversed(range(blocks)):
@@ -1304,71 +1314,105 @@
         step(2 * z)
         step(2 * z + 1)
 
+    def give(block, slot, target, h):
+        return pltpu.make_async_remote_copy(
+            src_ref=gathered.at[block, :, cuts[h]],
+            dst_ref=gathered.at[slot, :, cuts[h]],
+            send_sem=gs.at[slot, h],
+            recv_sem=gr.at[slot, h],
+            device_id={"tp": target},
+            device_id_type=MESH,
+        )
+
+    def share_out(h):
+        first = pl.multiple_of(col * quarter + h * (quarter // 2), quarter // 2)
+        own = d_ref[:, pl.ds(first, quarter // 2)].astype(jnp.float32)
+        gathered[0, :, cuts[h]] = (own + picked[:, cuts[h]]).astype(jnp.bfloat16)
+        given[(2, h)] = give(0, 2, far, h)
+        given[(1, h)] = give(0, 1, partner, h)
+        given[(2, h)].start()
+        given[(1, h)].start()
+
+    def share_on(h):
+        given[(2, h)].wait_recv()
+        given[(3, h)] = give(2, 3, partner, h)
+        given[(3, h)].start()
+
+    def settle(slot, h):
+        given[(slot, h)].wait_recv()
+
+    given = {}
     early = order[1:]
     gates(0)
     mixer_states()
     mixer_send(1, 0)
+    gates(early[0])
     arrive(1)
-    gates(early[0])
+    mixer_inner()
+    arrive(2 * early[0])
     complete(1)
     experts(0)
-    both(arrive, early[0])
+    arrive(2 * early[0] + 1)
     reduce_near(0)
-    for i, z in enumerate(early):
-        following = early[i + 1] if i + 1 < len(early) else None
-        if i == 0:
-            mixer_inner()
-        if following is not None:
-            gates(following)
+    gates(early[1])
+    both(relay, early[0])
+    both(complete, early[0])
+    experts(early[0])
+    for z in early[2:]:
+        both(arrive, z)
+    mixer_round(1)
+    reduce_near(early[0])
+    reduce_far(0)
+    both(arrive, early[1])
+    pending = [early[0]]
+    for i, z in enumerate(early[1:]):
+        following = early[i + 2] if i + 2 < len(early) else None
         both(relay, z)
         both(complete, z)
         experts(z)
+        mixer_round(1)
         if following is not None:
-            both(arrive, following)
+            gates(following)
+        if i > 0:
+            reduce_far(pending.pop(0))
         reduce_near(z)
-        if following is not None:
-            mixer_round(1)
-        reduce_far(order[i])
-    pick(0)
-    reduce_far(order[-1])
+        pending.append(z)
+    weight_grad(hidden, routed, wd_ref, grad_down)
+    reduce_far(pending.pop(0))
+    pick(0, 0)
+    pick(0, 1)
+    reduce_far(pending.pop(0))
+    weight_grad(d_gate, x_ref, wg_ref, grad_gate)
     while taken[0] < rounds:
         mixer_round(1)
     mixer_finish()
-    weight_grad(hidden, routed, wd_ref, grad_down)
+    weight_grad(d_up, x_ref, wu_ref, grad_up)
+    loads["w"].wait()
     for z in early:
-        pick(z)
-    own = d_ref[:, columns(col)].astype(jnp.float32)
-    gathered[0] = (own + picked[...]).astype(jnp.bfloat16)
-
-    def give(block, slot, target):
-        return pltpu.make_async_remote_copy(
-            src_ref=gathered.at[block],
-            dst_ref=gathered.at[slot],
-            send_sem=gs.at[slot],
-            recv_sem=gr.at[slot],
-            device_id={"tp": target},
-            device_id_type=MESH,
-        )
-
-    given = [give(0, 1, partner), give(0, 2, far), give(2, 3, partner)]
-    given[1].start()
-    given[0].start()
-    loads["w"].wait()
-    project(0)
+        pick(z, 0)
+    share_out(0)
+    project(0, 0)
+    for z in early:
+        pick(z, 1)
+    share_out(1)
+    project(0, 1)
     pair_up(0)
-    given[0].wait_recv()
-    project(1)
+    settle(1, 0)
+    project(1, 0)
+    settle(1, 1)
+    project(1, 1)
     pair_up(1)
-    weight_grad(d_gate, x_ref, wg_ref, grad_gate)
+    share_on(0)
+    project(2, 0)
     hand_over(0)
     hand_over(1)
-    weight_grad(d_up, x_ref, wu_ref, grad_up)
-    given[1].wait_recv()
-    given[2].start()
-    project(2)
+    share_on(1)
+    project(2, 1)
     pair_up(2)
-    given[2].wait_recv()
-    project(3)
+    settle(3, 0)
+    project(3, 0)
+    settle(3, 1)
+    project(3, 1)
     back_states()
     taken[0] = 0
     mixer_send(-1, 0)
@@ -1388,9 +1432,9 @@
     store(proj_ref, grad_proj)
     for copy in stored:
         copy.wait()
-    for copy in sent + given:
+    for copy in sent:
         copy.wait_send()
-    for group in (crossed, beside, relayed, halves, over, returned, paired_off):
+    for group in (given, crossed, beside, relayed, halves, over, returned, paired_off):
         for copy in group.values():
             copy.wait_send()
     for away, copy in handed:
@@ -1465,6 +1509,7 @@
             pltpu.VMEM((tokens, channels), bf16),
             pltpu.VMEM((tokens, channels), bf16),
             pltpu.VMEM((tokens, BLK), bf16),
+            pltpu.VMEM((tokens, width), f32),
             pltpu.VMEM((tokens, width), bf16),
             pltpu.VMEM((tokens, channels), f32),
             pltpu.VMEM((4, turns, 2, share, width), bf16),
@@ -1490,14 +1535,14 @@
             dma((n,)),
             dma((n // 2, 2)),
             dma((n // 2, 2)),
-            dma((n // 2,)),
-            dma((n // 2,)),
-            dma((n,)),
-            dma((n,)),
+            dma((n // 2, 2)),
+            dma((n // 2, 2)),
+            dma((n, 2)),
+            dma((n, 2)),
             dma((2 * rounds,)),
             dma((2 * rounds,)),
-            dma((4,)),
-            dma((4,)),
+            dma((4, 2)),
+            dma((4, 2)),
             dma((4, turns)),
             dma((4, turns)),
             dma((4, turns)),

time: 132 us -> 122 us (0.924)
  Pallas kernels: 131 us -> 121 us
    pallas_call x1, Pallas kernels: 123 us -> 114 us  [expert_stage(): pl.pallas_call(functools.partial(expert_kernel, n, cap, scale), out_shape...]
where the time goes in v1:
time: 122 us
  Pallas kernels  121 us (99%)
    pallas_call x1, Pallas kernels, expert_stage(): pl.pallas_call(functools.partial(expert_kernel, n, cap, scale), out_shape...  114 us
    pallas_call x1, Pallas kernels, store_out(): pl.pallas_call(functools.partial(store_kernel, pieces, count), out_shape=...  7.34 us

profile of v1, /device:TPU:3, one launch (start us, length us, event | category | flops | bytes accessed | tf_op | source)
XLA Modules:
  0.0 122.1 jit_solution(1561131604102974325)
XLA Ops:
  0.6 113.9 %expert_stage.1 = (bf16[704,2048]{1,0:T(8,128)(2,1)}, bf16[704,2048]{1,0:T(8,128)(2,1)}, bf16[704,2048]{1,0:T(8,128)(2,1)}, f32[256,256]{1,0:T(8,128)}, bf16[512...) custom-call(bf16[512,2048]{1,0:T(8,128)(2,1)} %d_hbm.1, ...), custom_call_target="tpu_custom_call" | custom-call | flops 60000002048 | bytes 30000000 | tf_op jit(solution)/shard_map/expert_stage/pallas_call | solution.py:1475
  114.5 7.3 %store_out.1 = (bf16[704,2048]{1,0:T(8,128)(2,1)}, bf16[704,2048]{1,0:T(8,128)(2,1)}, bf16[704,2048]{1,0:T(8,128)(2,1)}, f32[256,256]{1,0:T(8,128)}, bf16[512,12...) custom-call(bf16[704,2048]{1,0:T(8,128)(2,1)} %get-tuple-element.24.refs_0_, ...), custom_call_target="tpu_custom_call" | custom-call | tf_op jit(solution)/shard_map/store_out/pallas_call | solution.py:1591

commit v2 on v1

--- a/solution.py
+++ b/solution.py
@@ -1358,10 +1358,10 @@
     both(relay, early[0])
     both(complete, early[0])
     experts(early[0])
+    reduce_near(early[0])
     for z in early[2:]:
         both(arrive, z)
     mixer_round(1)
-    reduce_near(early[0])
     reduce_far(0)
     both(arrive, early[1])
     pending = [early[0]]

time: 122 us -> 126 us (1.033)
  Pallas kernels: 121 us -> 125 us
    pallas_call x1, Pallas kernels: 114 us -> 117 us  [expert_stage(): pl.pallas_call(functools.partial(expert_kernel, n, cap, scale), out_shape...]
where the time goes in v2:
time: 126 us
  Pallas kernels  125 us (99%)
    pallas_call x1, Pallas kernels, expert_stage(): pl.pallas_call(functools.partial(expert_kernel, n, cap, scale), out_shape...  117 us
    pallas_call x1, Pallas kernels, store_out(): pl.pallas_call(functools.partial(store_kernel, pieces, count), out_shape=...  7.34 us

profile of v2, /device:TPU:3, one launch (start us, length us, event | category | flops | bytes accessed | tf_op | source)
XLA Modules:
  0.0 125.6 jit_solution(17791755315020856869)
XLA Ops:
  0.6 117.4 %expert_stage.1 = (bf16[704,2048]{1,0:T(8,128)(2,1)}, bf16[704,2048]{1,0:T(8,128)(2,1)}, bf16[704,2048]{1,0:T(8,128)(2,1)}, f32[256,256]{1,0:T(8,128)}, bf16[512...) custom-call(bf16[512,2048]{1,0:T(8,128)(2,1)} %d_hbm.1, ...), custom_call_target="tpu_custom_call" | custom-call | flops 60000002048 | bytes 30000000 | tf_op jit(solution)/shard_map/expert_stage/pallas_call | solution.py:1475
  118.1 7.3 %store_out.1 = (bf16[704,2048]{1,0:T(8,128)(2,1)}, bf16[704,2048]{1,0:T(8,128)(2,1)}, bf16[704,2048]{1,0:T(8,128)(2,1)}, f32[256,256]{1,0:T(8,128)}, bf16[512,12...) custom-call(bf16[704,2048]{1,0:T(8,128)(2,1)} %get-tuple-element.24.refs_0_, ...), custom_call_target="tpu_custom_call" | custom-call | tf_op jit(solution)/shard_map/store_out/pallas_call | solution.py:1591
